TPU v7x, 256 devices: a whole 4x4x8 slice. The times are simulated.
256 devices in a mesh: ep: 16 (over y, x), tp: 16 (over z, core).
Axes of the slice: x: 4, y: 4, z: 8, core: 2. Of those that a mesh axis runs over, the one named last changes fastest.
Arguments:
- queries: bfloat16 [12288, 2048], P('ep', 'tp'), may hold values from -6 to 6
- keys: bfloat16 [12288, 512], P('ep'), may hold values from -6 to 6
- values: bfloat16 [12288, 512], P('ep'), may hold values from -6 to 6
- query_gain: float32 [128], replicated, may hold values from 1 to 4.5
- key_gain: float32 [128], replicated, may hold values from 1 to 4.5
- out_weight: bfloat16 [2048, 2048], P('tp'), may hold values from -0.75 to 0.75
- tokens_b: bfloat16 [12288, 2048], P('ep'), may hold values from -6 to 6
- norm_gain: float32 [2048], replicated, may hold values from 0.1 to 1.9
- routes: int32 [12288, 2], P('ep'), may hold values from 0 to 15, all different within a row; in each aligned block of 48 rows (0 to 47, 48 to 95, ...) at most 8 rows name the same one
- route_weight: float32 [12288, 2], P('ep'), may hold values from 0.2 to 1
- gate_weight: bfloat16 [16, 2048, 4096], P('ep', None, 'tp'), may hold values from -0.125 to 0.125
- up_weight: bfloat16 [16, 2048, 4096], P('ep', None, 'tp'), may hold values from -0.125 to 0.125
- down_weight: bfloat16 [16, 4096, 2048], P('ep', 'tp'), may hold values from -0.09375 to 0.09375
Outputs:
- mixed_out: bfloat16 [12288, 2048], P(('ep', 'tp'))
- expert_out: bfloat16 [12288, 2048], P(('ep', 'tp'))
Inputs may be any that keep to these rules, and one draw needn't show every extreme that they name: `routes`: A row names 2 different experts. In each aligned block of 48 rows no expert is named more than 8 times, a bound that some block reaches.
All inputs are finite; a program needn't handle non-finite values.
Results may differ from a plain program's by a relative error of at most 0.019.
Values may be sent and summed in bfloat16 or wider, within the bound.
A program may use at most 128 MiB of HBM per device.

v0:
```python
import jax
import jax.numpy as jnp
from jax import lax
from jax.sharding import Mesh
from jax.sharding import PartitionSpec as P

D = 2048
HD = 128
HQ = 16
KVH = 4
EXPERTS = 16
TOPK = 2
GRID_W = 64
CAP = 8
TP = ("tp_0", "tp_1")
EP_TP = ("ep", "tp_0", "tp_1")
EPS = 1e-06
THETA = 10000.0


def side_by_side(arrays, axis, dim, along):
    ends, at = ([], 0)
    for a in arrays[:-1]:
        at += a.shape[along]
        ends.append(at)
    both = jnp.concatenate(arrays, axis=along)
    return tuple(jnp.split(lax.all_gather(both, axis, axis=dim, tiled=True), ends, axis=along))


def sum_in_order(blocks, axes, sequence):
    inside = blocks.shape[1:]
    blocks = blocks.reshape(*(lax.axis_size(a) for a in axes), *inside)
    blocks = jnp.moveaxis(blocks, sequence, range(len(axes))).reshape(-1, *inside)
    for k in sequence:
        blocks = lax.psum_scatter(blocks, axes[k], scatter_dimension=0, tiled=True)
    return blocks[0]


def split_up(x, dim, size):
    before, after = (x.shape[:dim], x.shape[dim + 1 :])
    return jnp.moveaxis(x.reshape(*before, size, -1, *after), dim, 0)


def scatter_axes(x, axes, sequence, dim):
    size = lax.axis_size(axes)
    return sum_in_order(split_up(x, dim, size), axes, sequence)


def rotate(field, positions):
    n_freq = HD // 4
    row_pos = (positions // GRID_W).astype(jnp.float32)
    col_pos = (positions % GRID_W).astype(jnp.float32)
    inverse = THETA ** (-jnp.arange(n_freq, dtype=jnp.float32) / n_freq)
    angles = jnp.stack([row_pos[:, None] * inverse, col_pos[:, None] * inverse], axis=1)
    cosine = jnp.cos(angles)[:, None]
    sine = jnp.sin(angles)[:, None]
    length, n_heads = (field.shape[0], field.shape[1])
    halves = field.reshape(length, n_heads, 2, 2, n_freq)
    leading = halves[..., 0, :]
    second = halves[..., 1, :]
    turned = jnp.stack(
        [leading * cosine - second * sine, second * cosine + leading * sine], axis=-2
    )
    return turned.reshape(length, n_heads, HD)


def prepare(source, gain_vec, positions, n_heads):
    length = source.shape[0]
    field = source.astype(jnp.float32).reshape(length, n_heads, HD)
    field = field * lax.rsqrt(jnp.mean(field * field, axis=-1, keepdims=True) + EPS) * gain_vec
    return rotate(field, positions).astype(jnp.bfloat16)


def token_mixer(queries, keys, values, query_gain, key_gain, out_weight):
    n_rows = queries.shape[0]
    q_heads = queries.shape[1] // HD
    positions = lax.axis_index("ep") * n_rows + jnp.arange(n_rows, dtype=jnp.int32)
    query_n = prepare(queries, query_gain, positions, q_heads).reshape(n_rows * q_heads, HD)
    kv_index = lax.axis_index(TP) * q_heads // (HQ // KVH)
    own_keys = prepare(
        lax.dynamic_slice_in_dim(keys, kv_index * HD, HD, 1), key_gain, positions, 1
    ).reshape(n_rows, HD)
    own_values = lax.dynamic_slice_in_dim(values, kv_index * HD, HD, 1)
    score_scale = HD ** (-0.5)
    start_state = (
        jnp.full((n_rows * q_heads,), -1e30, jnp.float32),
        jnp.zeros((n_rows * q_heads,), jnp.float32),
        jnp.zeros((n_rows * q_heads, HD), jnp.float32),
    )
    key_piece, value_piece = side_by_side((own_keys, own_values), "ep", 0, 1)
    steps_n = key_piece.shape[0] // n_rows

    def one_block(index_b, state):
        running_max, totals, numerator = state
        key_blk = lax.dynamic_slice_in_dim(key_piece, index_b * n_rows, n_rows, 0)
        value_blk = lax.dynamic_slice_in_dim(value_piece, index_b * n_rows, n_rows, 0)
        scores = (
            jnp.einsum("qd,sd->qs", query_n, key_blk, preferred_element_type=jnp.float32)
            * score_scale
        )
        new_max = jnp.maximum(running_max, jnp.max(scores, axis=1))
        shrink = jnp.exp(running_max - new_max)
        weights = jnp.exp(scores - new_max[:, None])
        totals = totals * shrink + jnp.sum(weights, axis=1)
        numerator = numerator * shrink[:, None] + jnp.dot(
            weights.astype(jnp.bfloat16), value_blk, preferred_element_type=jnp.float32
        )
        return (new_max, totals, numerator)

    running_max, totals, numerator = lax.fori_loop(0, steps_n, one_block, start_state)
    attended = (numerator / totals[:, None]).astype(jnp.bfloat16)
    own_rows = lax.all_to_all(attended, TP, split_axis=0, concat_axis=1, tiled=True)
    return jnp.dot(
        own_rows,
        lax.all_gather(out_weight, TP, axis=0, tiled=True),
        preferred_element_type=jnp.float32,
    ).astype(jnp.bfloat16)


def expert_half(tokens_b, norm_gain, routes, route_weight, gate_weight, up_weight, down_weight):
    n_tp = lax.axis_size(TP)
    n_ep = lax.axis_size("ep")
    tp_index = lax.axis_index(TP)
    local_rows = tokens_b.shape[0]
    block_rows = local_rows // n_tp
    picks = block_rows * TOPK
    local_experts = gate_weight.shape[0]
    assigned = routes.reshape(n_tp, picks)
    onehot = (assigned[:, :, None] == jnp.arange(EXPERTS, dtype=jnp.int32)[None, None, :]).astype(
        jnp.int32
    )
    slot_rank = jnp.sum((jnp.cumsum(onehot, axis=1) - onehot) * onehot, axis=-1)
    target = assigned * CAP + slot_rank
    target_hot = (
        target[:, :, None] == jnp.arange(EXPERTS * CAP, dtype=jnp.int32)[None, None, :]
    ).astype(jnp.float32)
    token_hot = (
        jnp.arange(picks, dtype=jnp.int32)[:, None] // TOPK
        == jnp.arange(block_rows, dtype=jnp.int32)[None, :]
    ).astype(jnp.float32)
    own_block = lax.dynamic_slice_in_dim(tokens_b, tp_index * block_rows, block_rows, 0)
    field = own_block.astype(jnp.float32)
    own_normed = (
        field * lax.rsqrt(jnp.mean(field * field, axis=-1, keepdims=True) + EPS) * norm_gain
    ).astype(jnp.bfloat16)
    own_hot = lax.dynamic_index_in_dim(target_hot, tp_index, 0, keepdims=False)
    own_mat = jnp.einsum("aj,at->jt", own_hot, token_hot, precision=lax.Precision.HIGHEST).astype(
        jnp.bfloat16
    )
    outgoing = jnp.dot(own_mat, own_normed, preferred_element_type=jnp.float32)
    outgoing = outgoing.astype(jnp.bfloat16).reshape(EXPERTS, CAP, D)
    arrived = lax.all_to_all(outgoing, "ep", split_axis=0, concat_axis=1, tiled=True)
    arrived = arrived.reshape(1, local_experts, n_ep * CAP, D)
    slab_rows = lax.all_gather(arrived, TP, axis=0, tiled=True)
    gate_act = jnp.einsum(
        "blmd,ldf->blmf", slab_rows, gate_weight, preferred_element_type=jnp.float32
    )
    up_act = jnp.einsum("blmd,ldf->blmf", slab_rows, up_weight, preferred_element_type=jnp.float32)
    hidden = (jax.nn.silu(gate_act) * up_act).astype(jnp.bfloat16)
    result = jnp.einsum("blmf,lfd->blmd", hidden, down_weight, preferred_element_type=jnp.float32)
    terms = result.reshape(-1, D)
    summed = (
        scatter_axes(terms.astype(jnp.bfloat16), TP, (1, 0), 0)
        .astype(jnp.float32)
        .astype(jnp.bfloat16)
    )
    returned = lax.all_to_all(
        summed.reshape(local_experts, n_ep, CAP, D), "ep", split_axis=1, concat_axis=0, tiled=True
    )
    returned = returned.reshape(EXPERTS * CAP, D)
    own_target = lax.dynamic_index_in_dim(target_hot, tp_index, 0, keepdims=False)
    shares = (route_weight / jnp.sum(route_weight, axis=-1, keepdims=True)).reshape(n_tp, picks)
    own_shares = lax.dynamic_index_in_dim(shares, tp_index, 0, keepdims=False)
    combine = jnp.einsum(
        "at,aj->tj", token_hot, own_target * own_shares[:, None], precision=lax.Precision.HIGHEST
    )
    return jnp.dot(combine, returned.astype(jnp.float32), precision=lax.Precision.HIGHEST).astype(
        jnp.bfloat16
    )


def on_device(
    queries,
    keys,
    values,
    query_gain,
    key_gain,
    out_weight,
    tokens_b,
    norm_gain,
    routes,
    route_weight,
    gate_weight,
    up_weight,
    down_weight,
):
    mixed_out = token_mixer(queries, keys, values, query_gain, key_gain, out_weight)
    expert_out = expert_half(
        tokens_b, norm_gain, routes, route_weight, gate_weight, up_weight, down_weight
    )
    return (mixed_out, expert_out)


def solution(mesh):
    torus = Mesh(mesh.devices.reshape(mesh.shape["ep"], 8, 2), ("ep", "tp_0", "tp_1"))
    in_specs = (
        P("ep", TP),
        P("ep", None),
        P("ep", None),
        P(),
        P(),
        P(TP, None),
        P("ep", None),
        P(),
        P("ep", None),
        P("ep", None),
        P("ep", None, TP),
        P("ep", None, TP),
        P("ep", TP, None),
    )
    out_specs = (P(EP_TP, None), P(EP_TP, None))
    return jax.shard_map(
        on_device, mesh=torus, in_specs=in_specs, out_specs=out_specs, check_vma=False
    )
```

profile of v0, /device:TPU:1, one launch (start us, length us, event | category | flops | bytes accessed | tf_op | source)
XLA Modules:
  0.0 291.4 jit_solution(9098463858573012935)
XLA Ops:
  9.4 2.1 select_reduce_fusion
  14.6 17.9 %all_to_all.37 = bf16[16,8,2048]{2,1,0:T(8,128)(2,1)} all-to-all(bf16[16,8,2048]{2,1,0:T(8,128)(2,1)S(1)} %fusion.16), channel_id=1, replica_groups=mesh['ep'=16,'tp_0'=8,'tp_1'=2] {'ep'}, dimensions={0} | all-to-all | bytes 1048576 | tf_op jit(solution)/shard_map/all_to_all | solution.py:152
  32.6 56.8 %all-gather.8.cloned.1.call-done = bf16[16,1,128,2048]{3,2,1,0:T(8,128)(2,1)} async-done(((bf16[1,1,128,2048]{3,2,1,0:T(8,128)(2,1)}), bf16[16,1,128,2048]{3,2,1,0:T(8,128)(2,1)}) %all-gather.8.cloned.1.call-update) | async-done | bytes 8388624 | tf_op jit(solution)/shard_map/all_gather | solution.py:154
  89.4 7.1 %fusion.14 = f32[16,128,256]{2,1,0:T(8,128)} fusion(bf16[16,1,128,2048]{3,2,1,0:T(8,128)(2,1)} %all-gather.8.cloned.1.call-done, bf16[1,2048,256]{2,1,0:T(8,128)(2,1)S(1)} %copy-done.7), kind=kOutput, calls=%fused_computation.20 | convolution fusion | flops 2147483648 | bytes 11534336 | tf_op jit(solution)/shard_map/blmd,ldf->blmf/dot_general | solution.py:155
  96.5 13.2 %convolution_convert_fusion = bf16[16,128,2048]{2,1,0:T(8,128)(2,1)} fusion(bf16[16,1,128,2048]{3,2,1,0:T(8,128)(2,1)} %all-gather.8.cloned.1.call-done, f32[16,128,256]{2,1,0:T(8,128)} %fusion.14, bf16[1,256,2048]{2,1,0:T(8,128)(2,1)S(1)} %copy-done, bf16[1,2048,256]{2,1,0:T(8,128)(2,1)S(1)} %copy-done.8), kind=kOutput, calls=%fused_computation.22 | convolution fusion | flops 4302307328 | bytes 20971520 | tf_op jit(solution)/shard_map/blmf,lfd->blmd/dot_general | solution.py:160
  109.8 8.3 %copy.53 = bf16[8,2,128,2048]{3,2,0,1:T(8,128)(2,1)} copy(bf16[8,2,128,2048]{3,2,1,0:T(8,128)(2,1)} %bitcast.112) | data formatting | bytes 16777216 | tf_op jit(solution)/shard_map/convert_element_type | solution.py:163
  121.8 16.9 %reduce-scatter.3.cloned.1.call-done = bf16[8,128,2048]{2,1,0:T(8,128)(2,1)} async-done(((bf16[16,128,2048]{2,1,0:T(8,128)(2,1)}), bf16[8,128,2048]{2,1,0:T(8,128)(2,1)}) %reduce-scatter.3.cloned.1.call-update) | async-done | bytes 4194320 | tf_op jit(solution)/shard_map/reduce_scatter | solution.py:35
  139.6 46.2 %all-gather.4.cloned.1.call-done = bf16[12288,256]{0,1:T(8,128)(2,1)} async-done(((bf16[768,256]{0,1:T(8,128)(2,1)}), bf16[12288,256]{0,1:T(8,128)(2,1)}) %all-gather.4.cloned.1.call-update) | async-done | bytes 6291472 | tf_op jit(solution)/shard_map/all_gather | solution.py:27
  185.9 6.2 %fusion.74 = (bf16[12288,128]{0,1:T(8,128)(2,1)}, bf16[12288,128]{0,1:T(8,128)(2,1)}) fusion(bf16[12288,256]{0,1:T(8,128)(2,1)} %all-gather.4.cloned.1.call-done), kind=kLoop, calls=%fused_computation.121 | loop fusion | bytes 12582912 | tf_op jit(solution)/shard_map/split | solution.py:27
  192.1 55.9 %while.18 = (s32[]{:T(128)}, f32[768]{0:T(1024)S(1)}, f32[768]{0:T(1024)S(1)}, f32[768,128]{1,0:T(8,128)S(1)}, bf16[12288,128]{0,1:T(8,128)(2,1)}, /*index=5*/bf...) while((s32[]{:T(128)}, f32[768]{0:T(1024)S(1)}, ...), condition=%wide.region_5.6_spmd.clone, body=%wide.region_2.5_spmd.clone.sunk | while | flops 307007232 | bytes 8503471 | solution.py:110
  194.0 1.6 convolution_add_fusion.2
  197.5 1.6 convolution_add_fusion.2
  201.0 1.6 convolution_add_fusion.2
  204.5 1.6 convolution_add_fusion.2
  208.0 1.6 convolution_add_fusion.2
  209.6 1.5 multiply_reduce_fusion.2
  211.5 1.6 convolution_add_fusion.2
  215.0 1.6 convolution_add_fusion.2
  218.5 1.6 convolution_add_fusion.2
  222.0 1.6 convolution_add_fusion.2
  225.5 1.6 convolution_add_fusion.2
  229.0 1.6 convolution_add_fusion.2
  232.5 1.6 convolution_add_fusion.2
  236.0 1.6 convolution_add_fusion.2
  239.4 1.6 convolution_add_fusion.2
  242.9 1.6 convolution_add_fusion.2
  246.4 1.6 convolution_add_fusion.2
  248.9 8.0 %all-to-all-start = ((bf16[16,48,128]{2,1,0:T(8,128)(2,1)}), bf16[16,48,128]{2,1,0:T(8,128)(2,1)S(1)}, u32[]{:S(2)}, u32[]{:S(2)}) async-start(bf16[16,48,128]{2,1,0:T(8,128)(2,1)} %bitcast.6), calls=%async_computation | async-start | bytes 393216 | tf_op jit(solution)/shard_map/all_to_all | solution.py:112
  258.3 8.8 %all-to-all-done = bf16[16,48,128]{2,1,0:T(8,128)(2,1)S(1)} async-done(((bf16[16,48,128]{2,1,0:T(8,128)(2,1)}), bf16[16,48,128]{2,1,0:T(8,128)(2,1)S(1)}, u32[]{:S(2)}, u32[]{:S(2)}) %all-to-all-start) | async-done | bytes 196640 | tf_op jit(solution)/shard_map/all_to_all | solution.py:112
  267.0 4.9 %all-to-all-start.2 = ((bf16[1,16,8,2048]{3,2,0,1:T(8,128)(2,1)}), bf16[1,16,8,2048]{3,2,0,1:T(8,128)(2,1)S(1)}, u32[]{:S(2)}, u32[]{:S(2)}) async-start(bf16[1,16,8,2048]{3,2,0,1:T(8,128)(2,1)} %bitcast.118), calls=%async_computation.4 | async-start | bytes 1048576 | tf_op jit(solution)/shard_map/all_to_all | solution.py:167
  272.0 5.7 %convolution_convert_fusion.3 = bf16[48,2048]{1,0:T(8,128)(2,1)} fusion(bf16[2048,2048]{1,0:T(8,128)(2,1)} %all-gather.6.cloned.1.call-done, bf16[16,48,128]{2,1,0:T(8,128)(2,1)S(1)} %all-to-all-done), kind=kOutput, calls=%fused_computation.26 | convolution fusion | flops 402751488 | bytes 8781824 | tf_op jit(solution)/shard_map/dot_general | solution.py:113
  277.7 5.5 %all-to-all-done.2 = bf16[1,16,8,2048]{3,2,0,1:T(8,128)(2,1)S(1)} async-done(((bf16[1,16,8,2048]{3,2,0,1:T(8,128)(2,1)}), bf16[1,16,8,2048]{3,2,0,1:T(8,128)(2,1)S(1)}, u32[]{:S(2)}, u32[]{:S(2)}) %all-to-all-start.2) | async-done | bytes 524320 | tf_op jit(solution)/shard_map/all_to_all | solution.py:167
  (149 shorter events, 41.0 us)
Async XLA Ops:
  8.0 88.5 %copy-start = (bf16[1,256,2048]{2,1,0:T(8,128)(2,1)S(1)}, bf16[1,256,2048]{2,1,0:T(8,128)(2,1)}, u32[]{:S(2)}) copy-start(bf16[1,256,2048]{2,1,0:T(8,128)(2,1)} %param.27) | copy-start | bytes 3145732
  8.0 81.4 %copy-start.7 = (bf16[1,2048,256]{2,1,0:T(8,128)(2,1)S(1)}, bf16[1,2048,256]{2,1,0:T(8,128)(2,1)}, u32[]{:S(2)}) copy-start(bf16[1,2048,256]{2,1,0:T(8,128)(2,1)} %param.25) | copy-start | bytes 3145732
  8.0 81.4 %all-gather.8.cloned.1.call-start = ((), (), s32[]{:S(2)}) async-start(), calls=%async_computation.7 | async-start | bytes 8912896 | tf_op jit(solution)/shard_map/all_gather | solution.py:154
  11.9 84.6 %copy-start.3 = (pred[16,96,128]{2,1,0:T(32,128)(4,1)}, pred[16,96,128]{2,1,0:T(32,128)(4,1)S(1)}, u32[]{:S(2)}) copy-start(pred[16,96,128]{2,1,0:T(32,128)(4,1)S(1)} %iota_compare_fusion) | copy-start | bytes 589828
  32.5 64.0 %copy-start.8 = (bf16[1,2048,256]{2,1,0:T(8,128)(2,1)S(1)}, bf16[1,2048,256]{2,1,0:T(8,128)(2,1)}, u32[]{:S(2)}) copy-start(bf16[1,2048,256]{2,1,0:T(8,128)(2,1)} %param.26) | copy-start | bytes 3145732
  32.6 106.2 %reduce-scatter.3.cloned.1.call-start = ((), (), s32[]{:S(2)}) async-start(), calls=%async_computation.8 | async-start | bytes 12582912 | tf_op jit(solution)/shard_map/reduce_scatter | solution.py:35
  118.0 1.3 copy-start.2
  118.0 1.9 copy-start.5
  118.1 2.0 copy-start.6
  118.1 67.8 %all-gather.4.cloned.1.call-start = ((), (), s32[]{:S(2)}) async-start(), calls=%async_computation.5 | async-start | bytes 6684672 | tf_op jit(solution)/shard_map/all_gather | solution.py:27
  121.8 17.8 %copy-start.4 = (f32[768,2]{0,1:T(2,128)S(1)}, f32[768,2]{0,1:T(2,128)}, u32[]{:S(2)}) copy-start(f32[768,2]{0,1:T(2,128)} %param.24) | copy-start | bytes 18436
  121.8 145.2 %reduce-scatter.5.cloned.1.call-start = ((), (), s32[]{:S(2)}) async-start(), calls=%async_computation.9 | async-start | bytes 4718592 | tf_op jit(solution)/shard_map/reduce_scatter | solution.py:35
  138.8 133.2 %all-gather.6.cloned.1.call-start = ((), (), s32[]{:S(2)}) async-start(), calls=%async_computation.6 | async-start | bytes 8912896 | tf_op jit(solution)/shard_map/all_gather | solution.py:115
  248.9 18.2 %all-to-all-start = ((bf16[16,48,128]{2,1,0:T(8,128)(2,1)}), bf16[16,48,128]{2,1,0:T(8,128)(2,1)S(1)}, u32[]{:S(2)}, u32[]{:S(2)}) async-start(bf16[16,48,128]{2,1,0:T(8,128)(2,1)} %bitcast.6), calls=%async_computation | async-start | bytes 393216 | tf_op jit(solution)/shard_map/all_to_all | solution.py:112
  267.0 16.2 %all-to-all-start.2 = ((bf16[1,16,8,2048]{3,2,0,1:T(8,128)(2,1)}), bf16[1,16,8,2048]{3,2,0,1:T(8,128)(2,1)S(1)}, u32[]{:S(2)}, u32[]{:S(2)}) async-start(bf16[1,16,8,2048]{3,2,0,1:T(8,128)(2,1)} %bitcast.118), calls=%async_computation.4 | async-start | bytes 1048576 | tf_op jit(solution)/shard_map/all_to_all | solution.py:167
  272.0 12.3 %copy-start.1 = (bf16[1,256,2048]{2,1,0:T(8,128)(2,1)S(1)}, bf16[1,256,2048]{2,1,0:T(8,128)(2,1)}, u32[]{:S(2)}) copy-start(bf16[1,256,2048]{2,1,0:T(8,128)(2,1)} %param.27) | copy-start | bytes 3145732
Sparse Core Ops, SparseCore 0:
  32.7 56.7 all-gather.7
  118.2 20.5 reduce-scatter.2
  141.3 55.9 reduce-scatter.4
Sparse Core Ops, SparseCore 1:
  121.9 63.9 all-gather.3
  187.6 56.2 all-gather.5
where the time goes:
time: 293 us; the launch traced here: 291 us
  waiting for transfers between devices  135 us (46%)
  matrix products  77.6 us (26%)
  local copies, waits for them, and re-layouts  18 us (6%)
  blocking collectives  17.9 us (6%)
  between operations  15.5 us (5%)
  other arithmetic  13.6 us (5%)
  starting transfers between devices  13.3 us (5%)
    all_gather x1, waiting for transfers between devices, expert_half(): slab_rows = lax.all_gather(arrived, TP, axis=0, tiled=True)  56.8 us
    all_gather x1, waiting for transfers between devices, side_by_side(): lax.all_gather(both, axis, axis=dim, tiled=True)  46.2 us
    dot_general x16, matrix products, one_block(): jnp.dot(weights.astype(jnp.bfloat16), value_blk, preferred_element_type=j...  24.9 us
    dot_general x16, matrix products, one_block(): jnp.einsum('qd,sd->qs', query_n, key_blk, preferred_element_type=jnp.floa...  23 us
    all_to_all x1, blocking collectives, expert_half(): lax.all_to_all(outgoing, 'ep', split_axis=0, concat_axis=1, tiled=True)  17.9 us
    reduce_scatter x2, waiting for transfers between devices, sum_in_order(): blocks = lax.psum_scatter(blocks, axes[k], scatter_dimension=0, tiled=True)  16.9 us
    dot_general x1, matrix products, expert_half(): jnp.einsum('blmf,lfd->blmd', hidden, down_weight, preferred_element_type=...  13.2 us
    all_to_all x1, waiting for transfers between devices, token_mixer(): lax.all_to_all(attended, TP, split_axis=0, concat_axis=1, tiled=True)  8.78 us
  transfers between devices with their start and end apart: 7, of which 5 were waited for; matrix products, arithmetic and copies ran while one was open for 25% of the time, Pallas kernels for 0%

commit v1 on v0

--- a/solution.py
+++ b/solution.py
@@ -151,7 +151,9 @@
     outgoing = outgoing.astype(jnp.bfloat16).reshape(EXPERTS, CAP, D)
     arrived = lax.all_to_all(outgoing, "ep", split_axis=0, concat_axis=1, tiled=True)
     arrived = arrived.reshape(1, local_experts, n_ep * CAP, D)
-    slab_rows = lax.all_gather(arrived, TP, axis=0, tiled=True)
+    slab_rows = jnp.concatenate(
+        lax.all_to_all(jnp.stack([arrived] * lax.axis_size(TP)), TP, 0, 0), axis=0
+    )
     gate_act = jnp.einsum(
         "blmd,ldf->blmf", slab_rows, gate_weight, preferred_element_type=jnp.float32
     )

time: 293 us -> 428 us (1.46)
  blocking collectives: 17.9 us -> 214 us
  waiting for transfers between devices: 135 us -> 72.8 us
    all_to_all x0 -> x1, blocking collectives: none -> 196 us  [expert_half(): lax.all_to_all(jnp.stack([arrived] * lax.axis_size(TP)), TP, 0, 0)]
    all_gather x1 -> x0, waiting for transfers between devices: 56.8 us -> none  [expert_half(): slab_rows = lax.all_gather(arrived, TP, axis=0, tiled=True)]
    reduce_scatter x2, waiting for transfers between devices: 16.9 us -> 11.6 us  [sum_in_order(): blocks = lax.psum_scatter(blocks, axes[k], scatter_dimension=0, tiled=True)]
  transfers between devices with their start and end apart: 7 -> 6, of which waited for: 5 -> 4; matrix products, arithmetic and copies ran while one was open for 25% -> 17% of each run, Pallas kernels for 0% -> 0%
where the time goes in v1:
time: 428 us; the launch traced here: 427 us
  blocking collectives  214 us (50%)
  matrix products  74.2 us (17%)
  waiting for transfers between devices  72.8 us (17%)
  local copies, waits for them, and re-layouts  22.2 us (5%)
  between operations  15.8 us (4%)
  other arithmetic  13.5 us (3%)
  starting transfers between devices  13.2 us (3%)
    all_to_all x1, blocking collectives, expert_half(): lax.all_to_all(jnp.stack([arrived] * lax.axis_size(TP)), TP, 0, 0)  196 us
    all_gather x1, waiting for transfers between devices, side_by_side(): lax.all_gather(both, axis, axis=dim, tiled=True)  46.4 us
    dot_general x16, matrix products, one_block(): jnp.dot(weights.astype(jnp.bfloat16), value_blk, preferred_element_type=j...  24.9 us
    dot_general x16, matrix products, one_block(): jnp.einsum('qd,sd->qs', query_n, key_blk, preferred_element_type=jnp.floa...  23 us
    all_to_all x1, blocking collectives, expert_half(): lax.all_to_all(outgoing, 'ep', split_axis=0, concat_axis=1, tiled=True)  17.8 us
    dot_general x1, matrix products, expert_half(): jnp.einsum('blmf,lfd->blmd', hidden, down_weight, preferred_element_type=...  13.2 us
    reduce_scatter x2, waiting for transfers between devices, sum_in_order(): blocks = lax.psum_scatter(blocks, axes[k], scatter_dimension=0, tiled=True)  11.6 us
    all_to_all x1, waiting for transfers between devices, token_mixer(): lax.all_to_all(attended, TP, split_axis=0, concat_axis=1, tiled=True)  8.78 us
  transfers between devices with their start and end apart: 6, of which 4 were waited for; matrix products, arithmetic and copies ran while one was open for 17% of the time, Pallas kernels for 0%

profile of v1, /device:TPU:1, one launch (start us, length us, event | category | flops | bytes accessed | tf_op | source)
XLA Modules:
  0.0 426.6 jit_solution(6846863440759393902)
XLA Ops:
  9.3 2.1 select_reduce_fusion
  14.6 17.8 %all_to_all.42 = bf16[16,8,2048]{2,1,0:T(8,128)(2,1)S(1)} all-to-all(bf16[16,8,2048]{2,1,0:T(8,128)(2,1)S(1)} %fusion.16), channel_id=1, replica_groups=mesh['ep'=16,'tp_0'=8,'tp_1'=2] {'ep'}, dimensions={0} | all-to-all | bytes 1048576 | tf_op jit(solution)/shard_map/all_to_all | solution.py:152
  33.4 196.2 %all_to_all.43 = bf16[16,1,1,128,2048]{4,3,2,1,0:T(8,128)(2,1)S(1)} all-to-all(bf16[16,1,1,128,2048]{4,3,2,1,0:T(8,128)(2,1)S(1)} %stack.32), channel_id=1, replica_groups=mesh['ep'=16,'tp_0'=8,'tp_1'=2] {'tp_0','tp_1'}, dimensions={0} | all-to-all | bytes 16777216 | tf_op jit(solution)/shard_map/all_to_all | solution.py:155
  229.6 3.2 copy-done.2
  232.9 3.8 fusion.14
  236.6 13.2 %convolution_convert_fusion = bf16[16,128,2048]{2,1,0:T(8,128)(2,1)} fusion(bf16[16,1,1,128,2048]{4,3,2,1,0:T(8,128)(2,1)} %copy-done.2, f32[16,128,256]{2,1,0:T(8,128)} %fusion.14, bf16[1,256,2048]{2,1,0:T(8,128)(2,1)S(1)} %copy-done, bf16[1,2048,256]{2,1,0:T(8,128)(2,1)S(1)} %copy-done.9), kind=kOutput, calls=%fused_computation.22 | convolution fusion | flops 4302307328 | bytes 20971520 | tf_op jit(solution)/shard_map/blmf,lfd->blmd/dot_general | solution.py:162
  249.8 8.3 %copy.53 = bf16[8,2,128,2048]{3,2,0,1:T(8,128)(2,1)} copy(bf16[8,2,128,2048]{3,2,1,0:T(8,128)(2,1)} %bitcast.112) | data formatting | bytes 16777216 | tf_op jit(solution)/shard_map/convert_element_type | solution.py:165
  262.0 11.6 %reduce-scatter.3.cloned.1.call-done = bf16[8,128,2048]{2,1,0:T(8,128)(2,1)} async-done(((bf16[16,128,2048]{2,1,0:T(8,128)(2,1)}), bf16[8,128,2048]{2,1,0:T(8,128)(2,1)}) %reduce-scatter.3.cloned.1.call-update) | async-done | bytes 4194320 | tf_op jit(solution)/shard_map/reduce_scatter | solution.py:35
  274.5 46.4 %all-gather.3.cloned.1.call-done = bf16[12288,256]{0,1:T(8,128)(2,1)} async-done(((bf16[768,256]{0,1:T(8,128)(2,1)}), bf16[12288,256]{0,1:T(8,128)(2,1)}) %all-gather.3.cloned.1.call-update) | async-done | bytes 6291472 | tf_op jit(solution)/shard_map/all_gather | solution.py:27
  320.8 6.2 %fusion.74 = (bf16[12288,128]{0,1:T(8,128)(2,1)}, bf16[12288,128]{0,1:T(8,128)(2,1)}) fusion(bf16[12288,256]{0,1:T(8,128)(2,1)} %all-gather.3.cloned.1.call-done), kind=kLoop, calls=%fused_computation.121 | loop fusion | bytes 12582912 | tf_op jit(solution)/shard_map/split | solution.py:27
  327.0 55.9 %while.18 = (s32[]{:T(128)}, f32[768]{0:T(1024)S(1)}, f32[768]{0:T(1024)S(1)}, f32[768,128]{1,0:T(8,128)S(1)}, bf16[12288,128]{0,1:T(8,128)(2,1)}, /*index=5*/bf...) while((s32[]{:T(128)}, f32[768]{0:T(1024)S(1)}, ...), condition=%wide.region_5.6_spmd.clone, body=%wide.region_2.5_spmd.clone.sunk | while | flops 307007232 | bytes 8503471 | solution.py:110
  328.9 1.6 convolution_add_fusion.2
  332.4 1.6 convolution_add_fusion.2
  335.9 1.6 convolution_add_fusion.2
  339.4 1.6 convolution_add_fusion.2
  342.9 1.6 convolution_add_fusion.2
  346.4 1.6 convolution_add_fusion.2
  349.9 1.6 convolution_add_fusion.2
  353.4 1.6 convolution_add_fusion.2
  356.9 1.6 convolution_add_fusion.2
  360.4 1.6 convolution_add_fusion.2
  363.9 1.6 convolution_add_fusion.2
  367.4 1.6 convolution_add_fusion.2
  370.9 1.6 convolution_add_fusion.2
  374.4 1.6 convolution_add_fusion.2
  377.9 1.6 convolution_add_fusion.2
  381.4 1.6 convolution_add_fusion.2
  383.8 8.0 %all-to-all-start = ((bf16[16,48,128]{2,1,0:T(8,128)(2,1)}), bf16[16,48,128]{2,1,0:T(8,128)(2,1)S(1)}, u32[]{:S(2)}, u32[]{:S(2)}) async-start(bf16[16,48,128]{2,1,0:T(8,128)(2,1)} %bitcast.6), calls=%async_computation | async-start | bytes 393216 | tf_op jit(solution)/shard_map/all_to_all | solution.py:112
  393.2 8.8 %all-to-all-done = bf16[16,48,128]{2,1,0:T(8,128)(2,1)S(1)} async-done(((bf16[16,48,128]{2,1,0:T(8,128)(2,1)}), bf16[16,48,128]{2,1,0:T(8,128)(2,1)S(1)}, u32[]{:S(2)}, u32[]{:S(2)}) %all-to-all-start) | async-done | bytes 196640 | tf_op jit(solution)/shard_map/all_to_all | solution.py:112
  402.0 4.9 %all-to-all-start.3 = ((bf16[1,16,8,2048]{3,2,0,1:T(8,128)(2,1)}), bf16[1,16,8,2048]{3,2,0,1:T(8,128)(2,1)S(1)}, u32[]{:S(2)}, u32[]{:S(2)}) async-start(bf16[1,16,8,2048]{3,2,0,1:T(8,128)(2,1)} %bitcast.118), calls=%async_computation.5 | async-start | bytes 1048576 | tf_op jit(solution)/shard_map/all_to_all | solution.py:169
  407.0 5.7 %convolution_convert_fusion.3 = bf16[48,2048]{1,0:T(8,128)(2,1)} fusion(bf16[2048,2048]{1,0:T(8,128)(2,1)} %all-gather.5.cloned.1.call-done, bf16[16,48,128]{2,1,0:T(8,128)(2,1)S(1)} %all-to-all-done), kind=kOutput, calls=%fused_computation.26 | convolution fusion | flops 402751488 | bytes 8781824 | tf_op jit(solution)/shard_map/dot_general | solution.py:113
  412.7 5.5 %all-to-all-done.3 = bf16[1,16,8,2048]{3,2,0,1:T(8,128)(2,1)S(1)} async-done(((bf16[1,16,8,2048]{3,2,0,1:T(8,128)(2,1)}), bf16[1,16,8,2048]{3,2,0,1:T(8,128)(2,1)S(1)}, u32[]{:S(2)}, u32[]{:S(2)}) %all-to-all-start.3) | async-done | bytes 524320 | tf_op jit(solution)/shard_map/all_to_all | solution.py:169
  (150 shorter events, 43.5 us)
Async XLA Ops:
  8.0 228.6 %copy-start = (bf16[1,256,2048]{2,1,0:T(8,128)(2,1)S(1)}, bf16[1,256,2048]{2,1,0:T(8,128)(2,1)}, u32[]{:S(2)}) copy-start(bf16[1,256,2048]{2,1,0:T(8,128)(2,1)} %param.27) | copy-start | bytes 3145732
  8.0 265.6 %reduce-scatter.3.cloned.1.call-start = ((), (), s32[]{:S(2)}) async-start(), calls=%async_computation.8 | async-start | bytes 12582912 | tf_op jit(solution)/shard_map/reduce_scatter | solution.py:35
  11.8 21.6 %copy-start.4 = (pred[16,96,128]{2,1,0:T(32,128)(4,1)}, pred[16,96,128]{2,1,0:T(32,128)(4,1)S(1)}, u32[]{:S(2)}) copy-start(pred[16,96,128]{2,1,0:T(32,128)(4,1)S(1)} %iota_compare_fusion) | copy-start | bytes 589828
  33.4 199.4 %copy-start.8 = (bf16[1,2048,256]{2,1,0:T(8,128)(2,1)S(1)}, bf16[1,2048,256]{2,1,0:T(8,128)(2,1)}, u32[]{:S(2)}) copy-start(bf16[1,2048,256]{2,1,0:T(8,128)(2,1)} %param.25) | copy-start | bytes 3145732
  229.6 3.2 copy-start.2
  232.9 3.8 copy-start.9
  258.1 1.5 copy-start.3
  258.1 2.1 copy-start.6
  258.1 2.2 copy-start.7
  258.1 62.7 %all-gather.3.cloned.1.call-start = ((), (), s32[]{:S(2)}) async-start(), calls=%async_computation.6 | async-start | bytes 6684672 | tf_op jit(solution)/shard_map/all_gather | solution.py:27
  262.0 12.5 %copy-start.5 = (f32[768,2]{0,1:T(2,128)S(1)}, f32[768,2]{0,1:T(2,128)}, u32[]{:S(2)}) copy-start(f32[768,2]{0,1:T(2,128)} %param.24) | copy-start | bytes 18436
  262.0 140.0 %reduce-scatter.5.cloned.1.call-start = ((), (), s32[]{:S(2)}) async-start(), calls=%async_computation.9 | async-start | bytes 4718592 | tf_op jit(solution)/shard_map/reduce_scatter | solution.py:35
  273.6 133.3 %all-gather.5.cloned.1.call-start = ((), (), s32[]{:S(2)}) async-start(), calls=%async_computation.7 | async-start | bytes 8912896 | tf_op jit(solution)/shard_map/all_gather | solution.py:115
  383.8 18.2 %all-to-all-start = ((bf16[16,48,128]{2,1,0:T(8,128)(2,1)}), bf16[16,48,128]{2,1,0:T(8,128)(2,1)S(1)}, u32[]{:S(2)}, u32[]{:S(2)}) async-start(bf16[16,48,128]{2,1,0:T(8,128)(2,1)} %bitcast.6), calls=%async_computation | async-start | bytes 393216 | tf_op jit(solution)/shard_map/all_to_all | solution.py:112
  402.0 16.2 %all-to-all-start.3 = ((bf16[1,16,8,2048]{3,2,0,1:T(8,128)(2,1)}), bf16[1,16,8,2048]{3,2,0,1:T(8,128)(2,1)S(1)}, u32[]{:S(2)}, u32[]{:S(2)}) async-start(bf16[1,16,8,2048]{3,2,0,1:T(8,128)(2,1)} %bitcast.118), calls=%async_computation.5 | async-start | bytes 1048576 | tf_op jit(solution)/shard_map/all_to_all | solution.py:169
  406.9 12.3 %copy-start.1 = (bf16[1,256,2048]{2,1,0:T(8,128)(2,1)S(1)}, bf16[1,256,2048]{2,1,0:T(8,128)(2,1)}, u32[]{:S(2)}) copy-start(bf16[1,256,2048]{2,1,0:T(8,128)(2,1)} %param.27) | copy-start | bytes 3145732
Sparse Core Ops, SparseCore 0:
  258.2 15.3 reduce-scatter.2
  276.1 55.9 reduce-scatter.4
Sparse Core Ops, SparseCore 1:
  262.1 58.7 all-gather.2
  322.5 56.2 all-gather.4
